TPU v7x, 32 devices: a whole 2x2x4 slice. The times are simulated.
32 devices in a mesh: fs: 16 (over z, y, x), tp: 2 (over core).
Axes of the slice: x: 2, y: 2, z: 4, core: 2. Of those that a mesh axis runs over, the one named last changes fastest.
Arguments:
- tokens: bfloat16 [8192, 2048], P('fs', 'tp'), may hold values from -24 to 24
- u_weight: bfloat16 [2048, 1024], P('fs', 'tp'), may hold values from -0.125 to 0.125
- v_weight: bfloat16 [2048, 1024], P('fs', 'tp'), may hold values from -0.125 to 0.125
- sg_gain: float32 [1024], P('tp'), may hold values from 0.1 to 1.9
- spatial_weight: bfloat16 [8, 128, 128], P('tp'), may hold values from -0.5 to 0.5
- spatial_bias: float32 [8, 128], P('tp'), may hold values from 0.1 to 1.9
- out_weight: bfloat16 [1024, 2048], P('tp', 'fs'), may hold values from -0.1875 to 0.1875
- gain_one: float32 [2048], P('tp'), may hold values from 0.1 to 1.9
- gate_weight: bfloat16 [2048, 5632], P('fs', 'tp'), may hold values from -0.125 to 0.125
- up_weight: bfloat16 [2048, 5632], P('fs', 'tp'), may hold values from -0.125 to 0.125
- down_weight: bfloat16 [5632, 2048], P('tp', 'fs'), may hold values from -0.078125 to 0.078125
- gain_two: float32 [2048], P('tp'), may hold values from 0.1 to 1.9
Outputs:
- layer_out: bfloat16 [8192, 2048], P('fs', 'tp')
All inputs are finite; a program needn't handle non-finite values.
Results may differ from a plain program's by a relative error of at most 0.014.
Values may be sent and summed in bfloat16 or wider, within the bound.
A program may use at most 128 MiB of HBM per device.

v0:
```python
import jax
import jax.numpy as jnp
from jax import lax
from jax.sharding import PartitionSpec as P

EPS = 1e-05
ALPHA = 2.0**0.25


def add_rows(left, piece):
    return jnp.dot(left, piece, preferred_element_type=jnp.float32)


def scaled_rows(vals, sums, gain, count):
    mean = sums[0][:, None] / count
    square = sums[1][:, None] / count
    return (vals - mean) * lax.rsqrt(square - mean * mean + EPS) * gain[None, :]


def on_device(
    tokens,
    u_weight,
    v_weight,
    sg_gain,
    spatial_weight,
    spatial_bias,
    out_weight,
    gain_one,
    gate_weight,
    up_weight,
    down_weight,
    gain_two,
):
    parts = lax.axis_size("tp")
    whole = lax.all_gather(tokens, "tp", axis=1, tiled=True)
    rows = whole.shape[0]
    width_sg = u_weight.shape[1]

    def add_one(piece):
        return add_rows(whole, piece)

    pre_u = add_one(lax.all_gather(u_weight, "fs", axis=0, tiled=True))
    pre_v = add_one(lax.all_gather(v_weight, "fs", axis=0, tiled=True))
    gated = jax.nn.gelu(pre_u)
    valued = jax.nn.gelu(pre_v)
    stats = lax.psum((jnp.sum(valued, axis=1), jnp.sum(valued * valued, axis=1)), "tp")
    normed = scaled_rows(valued, stats, sg_gain, width_sg * parts).astype(jnp.bfloat16)
    groups_here = spatial_weight.shape[0]
    block = spatial_weight.shape[1]
    group_width = width_sg // groups_here
    shaped = normed.reshape(rows // block, block, groups_here, group_width)
    lower = jnp.tril(jnp.ones((block, block), jnp.bool_))
    masked = jnp.where(lower[None], spatial_weight, jnp.zeros_like(spatial_weight))
    mixed = jnp.einsum("gij,njgd->nigd", masked, shaped, preferred_element_type=jnp.float32)
    mixed = mixed + spatial_bias.T[None, :, :, None]
    gated_out = (gated * mixed.reshape(rows, width_sg)).astype(jnp.bfloat16)
    terms = jnp.dot(
        gated_out,
        lax.all_gather(out_weight, "fs", axis=1, tiled=True),
        preferred_element_type=jnp.float32,
    )
    mix = lax.psum_scatter(terms.astype(jnp.bfloat16), "tp", scatter_dimension=1, tiled=True)
    resid = ALPHA * tokens.astype(jnp.float32) + mix.astype(jnp.float32)
    first_sums = lax.psum((jnp.sum(resid, axis=1), jnp.sum(resid * resid, axis=1)), "tp")
    first = scaled_rows(resid, first_sums, gain_one, resid.shape[1] * parts).astype(jnp.bfloat16)
    whole_first = lax.all_gather(first, "tp", axis=1, tiled=True)

    def add_first(piece):
        return add_rows(whole_first, piece)

    gate = add_first(lax.all_gather(gate_weight, "fs", axis=0, tiled=True))
    upper = add_first(lax.all_gather(up_weight, "fs", axis=0, tiled=True))
    hidden = (jax.nn.silu(gate) * upper).astype(jnp.bfloat16)
    ffn_terms = jnp.dot(
        hidden,
        lax.all_gather(down_weight, "fs", axis=1, tiled=True),
        preferred_element_type=jnp.float32,
    )
    ffn = lax.psum_scatter(ffn_terms.astype(jnp.bfloat16), "tp", scatter_dimension=1, tiled=True)
    second = ALPHA * first.astype(jnp.float32) + ffn.astype(jnp.float32)
    last_sums = lax.psum((jnp.sum(second, axis=1), jnp.sum(second * second, axis=1)), "tp")
    return scaled_rows(second, last_sums, gain_two, second.shape[1] * parts).astype(jnp.bfloat16)


def solution(mesh):
    return jax.shard_map(
        on_device,
        mesh=mesh,
        in_specs=(
            P("fs", "tp"),
            P("fs", "tp"),
            P("fs", "tp"),
            P("tp"),
            P("tp", None, None),
            P("tp", None),
            P("tp", "fs"),
            P("tp"),
            P("fs", "tp"),
            P("fs", "tp"),
            P("tp", "fs"),
            P("tp"),
        ),
        out_specs=P("fs", "tp"),
        check_vma=False,
    )
```

profile of v0, /device:TPU:0, one launch (start us, length us, event | category | flops | bytes accessed | tf_op | source)
XLA Modules:
  0.0 759.9 jit_solution(2212430606449240204)
XLA Ops:
  6.5 0.7 all-gather.9.cloned.1.call-update
  9.4 12.8 %all-gather.9.cloned.1.call-done = bf16[512,2048]{1,0:T(8,128)(2,1)} async-done(((bf16[512,1024]{1,0:T(8,128)(2,1)}), bf16[512,2048]{1,0:T(8,128)(2,1)}) %all-gather.9.cloned.1.call-update) | async-done | bytes 2097168 | tf_op jit(solution)/shard_map/all_gather | solution.py:35
  22.2 64.4 %all-gather.13.cloned.1.call-done = bf16[2048,512]{1,0:T(8,128)(2,1)} async-done(((bf16[128,512]{1,0:T(8,128)(2,1)}), bf16[2048,512]{1,0:T(8,128)(2,1)}) %all-gather.13.cloned.1.call-update) | async-done | bytes 2097168 | tf_op jit(solution)/shard_map/all_gather | solution.py:43
  86.6 3.8 fusion.35
  90.4 2.6 all-reduce.2
  94.4 54.1 %all-gather.11.cloned.1.call-done = bf16[2048,512]{1,0:T(8,128)(2,1)} async-done(((bf16[128,512]{1,0:T(8,128)(2,1)}), bf16[2048,512]{1,0:T(8,128)(2,1)}) %all-gather.11.cloned.1.call-update) | async-done | bytes 2097168 | tf_op jit(solution)/shard_map/all_gather | solution.py:42
  148.5 64.3 %all-gather.15.cloned.1.call-done = bf16[512,2048]{1,0:T(8,128)(2,1)} async-done(((bf16[512,128]{1,0:T(8,128)(2,1)}), bf16[512,2048]{1,0:T(8,128)(2,1)}) %all-gather.15.cloned.1.call-update) | async-done | bytes 2097168 | tf_op jit(solution)/shard_map/all_gather | solution.py:59
  212.9 6.8 convolution_convert_fusion.1
  219.7 7.9 %reduce-scatter.3.cloned.1.call-done = bf16[512,1024]{1,0:T(8,128)(2,1)} async-done(((bf16[512,2048]{1,0:T(8,128)(2,1)}), bf16[512,1024]{1,0:T(8,128)(2,1)}) %reduce-scatter.3.cloned.1.call-update) | async-done | bytes 1048592 | tf_op jit(solution)/shard_map/reduce_scatter | solution.py:62
  227.6 1.9 fusion
  229.5 2.5 all-reduce.1
  232.0 1.5 multiply_convert_fusion.2
  233.6 0.7 all-gather.19.cloned.1.call-update
  234.4 0.7 all-gather.21.cloned.1.call-update
  236.1 9.5 %all-gather.17.cloned.1.call-done = bf16[512,2048]{1,0:T(8,128)(2,1)} async-done(((bf16[512,1024]{1,0:T(8,128)(2,1)}), bf16[512,2048]{1,0:T(8,128)(2,1)}) %all-gather.17.cloned.1.call-update) | async-done | bytes 2097168 | tf_op jit(solution)/shard_map/all_gather | solution.py:66
  245.6 145.4 %all-gather.19.cloned.1.call-done = bf16[2048,2816]{1,0:T(8,128)(2,1)} async-done(((bf16[128,2816]{1,0:T(8,128)(2,1)}), bf16[2048,2816]{1,0:T(8,128)(2,1)}) %all-gather.19.cloned.1.call-update) | async-done | bytes 11534352 | tf_op jit(solution)/shard_map/all_gather | solution.py:71
  391.0 12.5 %fusion.38 = f32[512,2816]{1,0:T(8,128)} fusion(bf16[512,2048]{1,0:T(8,128)(2,1)} %all-gather.17.cloned.1.call-done, bf16[2048,2816]{1,0:T(8,128)(2,1)} %all-gather.19.cloned.1.call-done), kind=kOutput, calls=%fused_computation.57 | convolution fusion | flops 5905580032 | bytes 19398656 | tf_op jit(solution)/shard_map/dot_general | solution.py:11
  403.5 129.9 %all-gather.21.cloned.1.call-done = bf16[2048,2816]{1,0:T(8,128)(2,1)} async-done(((bf16[128,2816]{1,0:T(8,128)(2,1)}), bf16[2048,2816]{1,0:T(8,128)(2,1)}) %all-gather.21.cloned.1.call-update) | async-done | bytes 11534352 | tf_op jit(solution)/shard_map/all_gather | solution.py:72
  533.4 183.0 %all-gather.23.cloned.1.call-done = bf16[2816,2048]{1,0:T(8,128)(2,1)} async-done(((bf16[2816,128]{1,0:T(8,128)(2,1)}), bf16[2816,2048]{1,0:T(8,128)(2,1)}) %all-gather.23.cloned.1.call-update) | async-done | bytes 11534352 | tf_op jit(solution)/shard_map/all_gather | solution.py:76
  716.4 22.8 %convolution_convert_fusion = bf16[512,2048]{1,0:T(8,128)(2,1)} fusion(bf16[2816,2048]{1,0:T(8,128)(2,1)} %all-gather.23.cloned.1.call-done, f32[512,2816]{1,0:T(8,128)} %fusion.38, bf16[512,2048]{1,0:T(8,128)(2,1)S(1)} %copy-done.9, bf16[2048,2816]{1,0:T(8,128)(2,1)} %all-gather.21.cloned.1.call-done), kind=kOutput, calls=%fused_computation.1 | convolution fusion | flops 11820859392 | bytes 33030144 | tf_op jit(solution)/shard_map/dot_general | solution.py:74
  739.2 8.0 %reduce-scatter.5.cloned.1.call-done = bf16[512,1024]{1,0:T(8,128)(2,1)} async-done(((bf16[512,2048]{1,0:T(8,128)(2,1)}), bf16[512,1024]{1,0:T(8,128)(2,1)}) %reduce-scatter.5.cloned.1.call-update) | async-done | bytes 1048592 | tf_op jit(solution)/shard_map/reduce_scatter | solution.py:79
  747.1 1.9 fusion.1
  749.0 2.5 all-reduce
  751.5 1.5 multiply_convert_fusion.1
  (45 shorter events, 4.6 us)
Async XLA Ops:
  6.5 15.7 %all-gather.9.cloned.1.call-start = ((), (), s32[]{:S(2)}) async-start(), calls=%async_computation.2 | async-start | bytes 3145728 | tf_op jit(solution)/shard_map/all_gather | solution.py:35
  7.3 79.3 %all-gather.13.cloned.1.call-start = ((), (), s32[]{:S(2)}) async-start(), calls=%async_computation.4 | async-start | bytes 2228224 | tf_op jit(solution)/shard_map/all_gather | solution.py:43
  8.0 140.5 %all-gather.11.cloned.1.call-start = ((), (), s32[]{:S(2)}) async-start(), calls=%async_computation.3 | async-start | bytes 2228224 | tf_op jit(solution)/shard_map/all_gather | solution.py:42
  8.7 204.1 %all-gather.15.cloned.1.call-start = ((), (), s32[]{:S(2)}) async-start(), calls=%async_computation.5 | async-start | bytes 2228224 | tf_op jit(solution)/shard_map/all_gather | solution.py:59
  9.3 218.3 %reduce-scatter.3.cloned.1.call-start = ((), (), s32[]{:S(2)}) async-start(), calls=%async_computation.6 | async-start | bytes 3145728 | tf_op jit(solution)/shard_map/reduce_scatter | solution.py:62
  9.4 83.7 %copy-start.7 = (f32[512]{0:T(512)S(1)}, f32[512]{0:T(512)}, u32[]{:S(2)}) copy-start(f32[512]{0:T(512)} %param.15) | copy-start | bytes 6148
  90.4 3.2 copy-start.4
  90.4 3.2 copy-start.8
  219.7 8.0 %copy-start.1 = (bf16[512,1024]{1,0:T(8,128)(2,1)S(1)}, bf16[512,1024]{1,0:T(8,128)(2,1)}, u32[]{:S(2)}) copy-start(bf16[512,1024]{1,0:T(8,128)(2,1)} %param.12) | copy-start | bytes 3145732
  219.7 12.4 %copy-start.5 = (f32[1024]{0:T(1024)S(1)}, f32[1024]{0:T(1024)}, u32[]{:S(2)}) copy-start(f32[1024]{0:T(1024)} %param.19) | copy-start | bytes 12292
  219.7 25.9 %all-gather.17.cloned.1.call-start = ((), (), s32[]{:S(2)}) async-start(), calls=%async_computation.7 | async-start | bytes 3145728 | tf_op jit(solution)/shard_map/all_gather | solution.py:66
  227.6 4.4 copy-start.2
  233.6 157.4 %all-gather.19.cloned.1.call-start = ((), (), s32[]{:S(2)}) async-start(), calls=%async_computation.8 | async-start | bytes 12255232 | tf_op jit(solution)/shard_map/all_gather | solution.py:71
  234.3 299.1 %all-gather.21.cloned.1.call-start = ((), (), s32[]{:S(2)}) async-start(), calls=%async_computation.9 | async-start | bytes 12255232 | tf_op jit(solution)/shard_map/all_gather | solution.py:72
  235.1 481.3 %all-gather.23.cloned.1.call-start = ((), (), s32[]{:S(2)}) async-start(), calls=%async_computation.10 | async-start | bytes 12255232 | tf_op jit(solution)/shard_map/all_gather | solution.py:76
  235.8 511.3 %reduce-scatter.5.cloned.1.call-start = ((), (), s32[]{:S(2)}) async-start(), calls=%async_computation.11 | async-start | bytes 3145728 | tf_op jit(solution)/shard_map/reduce_scatter | solution.py:79
  245.6 470.8 %copy-start.9 = (bf16[512,2048]{1,0:T(8,128)(2,1)S(1)}, bf16[512,2048]{1,0:T(8,128)(2,1)}, u32[]{:S(2)}) copy-start(bf16[512,2048]{1,0:T(8,128)(2,1)} %all-gather.17.cloned.1.call-done) | copy-start | bytes 6291460
  739.1 8.0 %copy-start = (bf16[512,1024]{1,0:T(8,128)(2,1)S(1)}, bf16[512,1024]{1,0:T(8,128)(2,1)}, u32[]{:S(2)}) copy-start(bf16[512,1024]{1,0:T(8,128)(2,1)} %multiply_convert_fusion.2) | copy-start | bytes 3145732
  739.1 12.4 %copy-start.6 = (f32[1024]{0:T(1024)S(1)}, f32[1024]{0:T(1024)}, u32[]{:S(2)}) copy-start(f32[1024]{0:T(1024)} %param.23) | copy-start | bytes 12292
  747.1 4.4 copy-start.3
Sparse Core Ops, SparseCore 0:
  8.9 13.2 all-gather.8
  25.0 61.5 all-gather.12
  89.3 59.1 all-gather.10
  151.1 61.7 all-gather.14
  219.8 7.7 reduce-scatter.2
  233.7 11.8 all-gather.16
  248.3 142.5 all-gather.18
  393.7 139.6 all-gather.20
  536.1 180.2 all-gather.22
  739.3 7.7 reduce-scatter.4
where the time goes:
time: 760 us
  waiting for transfers between devices  684 us (90%)
  matrix products  46.3 us (6%)
  between operations  13.6 us (2%)
    all_gather x1, waiting for transfers between devices, on_device(): lax.all_gather(down_weight, 'fs', axis=1, tiled=True)  183 us
    all_gather x1, waiting for transfers between devices, on_device(): gate = add_first(lax.all_gather(gate_weight, 'fs', axis=0, tiled=True))  145 us
    all_gather x1, waiting for transfers between devices, on_device(): upper = add_first(lax.all_gather(up_weight, 'fs', axis=0, tiled=True))  130 us
    all_gather x1, waiting for transfers between devices, on_device(): pre_v = add_one(lax.all_gather(v_weight, 'fs', axis=0, tiled=True))  64.4 us
    all_gather x1, waiting for transfers between devices, on_device(): lax.all_gather(out_weight, 'fs', axis=1, tiled=True)  64.3 us
    all_gather x1, waiting for transfers between devices, on_device(): pre_u = add_one(lax.all_gather(u_weight, 'fs', axis=0, tiled=True))  54.1 us
    dot_general x1, matrix products, on_device(): jnp.dot(hidden, lax.all_gather(down_weight, 'fs', axis=1, tiled=True), pr...  22.8 us
    dot_general x2, matrix products, add_rows(): return jnp.dot(left, piece, preferred_element_type=jnp.float32)  16.3 us
  transfers between devices with their start and end apart: 10, of which 10 were waited for; matrix products, arithmetic and copies ran while one was open for 2% of the time, Pallas kernels for 0%

commit v1 on v0

--- a/solution.py
+++ b/solution.py
@@ -1,3 +1,4 @@
+import functools
 import jax
 import jax.numpy as jnp
 from jax import lax
@@ -5,6 +6,24 @@
 
 EPS = 1e-05
 ALPHA = 2.0**0.25
+
+
+def bind_sections(xs, named_axis):
+    work_now = lax.axis_index(named_axis)
+    side_arr = lax.axis_size(named_axis)
+    val2, x_new, v_now = (side_arr, work_now, xs.shape[0])
+    z_new, long_array = (xs, 1)
+    while long_array < val2:
+        stack_in = []
+        for dd in range(val2):
+            stack_in.append((dd, (dd - long_array) % val2))
+        y_new = lax.ppermute(z_new, named_axis, stack_in)
+        z_new = jnp.concatenate([z_new, y_new], axis=0)
+        long_array = 2 * long_array
+    return jnp.roll(z_new, x_new * v_now, axis=0)
+
+
+search_the_trees = functools.partial(bind_sections, named_axis="fs")
 
 
 def add_rows(left, piece):
@@ -39,7 +58,7 @@
     def add_one(piece):
         return add_rows(whole, piece)
 
-    pre_u = add_one(lax.all_gather(u_weight, "fs", axis=0, tiled=True))
+    pre_u = add_one(search_the_trees(u_weight))
     pre_v = add_one(lax.all_gather(v_weight, "fs", axis=0, tiled=True))
     gated = jax.nn.gelu(pre_u)
     valued = jax.nn.gelu(pre_v)

time: 760 us -> 733 us (0.964)
  waiting for transfers between devices: 684 us -> 638 us
  starting transfers between devices: 0.53 us -> 9.59 us
  local copies, waits for them, and re-layouts: 0.57 us -> 8.75 us
    ppermute x0 -> x4, waiting for transfers between devices: none -> 70.6 us  [bind_sections(): y_new = lax.ppermute(z_new, named_axis, stack_in)]
    all_gather x1 -> x0, waiting for transfers between devices: 54.1 us -> none  [on_device(): pre_u = add_one(lax.all_gather(u_weight, 'fs', axis=0, tiled=True))]
    all_gather x1, waiting for transfers between devices: 64.4 us -> 24.3 us  [on_device(): pre_v = add_one(lax.all_gather(v_weight, 'fs', axis=0, tiled=True))]
    all_gather x1, waiting for transfers between devices: 12.8 us -> 0.01 us  [on_device(): whole = lax.all_gather(tokens, 'tp', axis=1, tiled=True)]
    ppermute x0 -> x4, starting transfers between devices: none -> 9.09 us  [bind_sections(): y_new = lax.ppermute(z_new, named_axis, stack_in)]
    all_gather x1, waiting for transfers between devices: 64.3 us -> 56.4 us  [on_device(): lax.all_gather(out_weight, 'fs', axis=1, tiled=True)]
  transfers between devices with their start and end apart: 10 -> 13, of which waited for: 10 -> 12; matrix products, arithmetic and copies ran while one was open for 2% -> 4% of each run, Pallas kernels for 0% -> 0%
where the time goes in v1:
time: 733 us
  waiting for transfers between devices  638 us (87%)
  matrix products  46.3 us (6%)
  between operations  13.3 us (2%)
  starting transfers between devices  9.59 us (1%)
  other arithmetic  9.26 us (1%)
  local copies, waits for them, and re-layouts  8.75 us (1%)
  blocking collectives  7.54 us (1%)
    all_gather x1, waiting for transfers between devices, on_device(): lax.all_gather(down_weight, 'fs', axis=1, tiled=True)  183 us
    all_gather x1, waiting for transfers between devices, on_device(): gate = add_first(lax.all_gather(gate_weight, 'fs', axis=0, tiled=True))  145 us
    all_gather x1, waiting for transfers between devices, on_device(): upper = add_first(lax.all_gather(up_weight, 'fs', axis=0, tiled=True))  130 us
    ppermute x4, waiting for transfers between devices, bind_sections(): y_new = lax.ppermute(z_new, named_axis, stack_in)  70.6 us
    all_gather x1, waiting for transfers between devices, on_device(): lax.all_gather(out_weight, 'fs', axis=1, tiled=True)  56.4 us
    all_gather x1, waiting for transfers between devices, on_device(): pre_v = add_one(lax.all_gather(v_weight, 'fs', axis=0, tiled=True))  24.3 us
    dot_general x1, matrix products, on_device(): jnp.dot(hidden, lax.all_gather(down_weight, 'fs', axis=1, tiled=True), pr...  22.8 us
    dot_general x2, matrix products, add_rows(): return jnp.dot(left, piece, preferred_element_type=jnp.float32)  16.3 us
  transfers between devices with their start and end apart: 13, of which 12 were waited for; matrix products, arithmetic and copies ran while one was open for 4% of the time, Pallas kernels for 0%

profile of v1, /device:TPU:0, one launch (start us, length us, event | category | flops | bytes accessed | tf_op | source)
XLA Modules:
  0.0 733.2 jit_solution(17388380341607111629)
XLA Ops:
  8.1 7.0 collective-permute-start
  15.1 3.1 collective-permute-done
  20.6 5.7 collective-permute-done.1
  27.8 12.4 %collective-permute-done.2 = bf16[512,512]{1,0:T(8,128)(2,1)S(1)} collective-permute-done((bf16[512,512]{1,0:T(8,128)(2,1)S(1)}, bf16[512,512]{1,0:T(8,128)(2,1)S(1)}, u32[]{:S(2)}, u32[]{:S(2)}) %collective-permute-start.2) | collective-permute-done | bytes 524320 | tf_op jit(solution)/shard_map/ppermute | solution.py:20
  43.3 49.4 %collective-permute-done.3 = bf16[1024,512]{1,0:T(8,128)(2,1)S(1)} collective-permute-done((bf16[1024,512]{1,0:T(8,128)(2,1)S(1)}, bf16[1024,512]{1,0:T(8,128)(2,1)S(1)}, u32[]{:S(2)}, u32[]{:S(2)}) %collective-permute-start.3) | collective-permute-done | bytes 1048608 | tf_op jit(solution)/shard_map/ppermute | solution.py:20
  97.7 24.3 %all-gather.10.cloned.1.call-done = bf16[2048,512]{1,0:T(8,128)(2,1)} async-done(((bf16[128,512]{1,0:T(8,128)(2,1)}), bf16[2048,512]{1,0:T(8,128)(2,1)}) %all-gather.10.cloned.1.call-update) | async-done | bytes 2097168 | tf_op jit(solution)/shard_map/all_gather | solution.py:62
  122.1 3.8 fusion.49
  125.9 2.6 all-reduce.2
  130.1 56.4 %all-gather.12.cloned.1.call-done = bf16[512,2048]{1,0:T(8,128)(2,1)} async-done(((bf16[512,128]{1,0:T(8,128)(2,1)}), bf16[512,2048]{1,0:T(8,128)(2,1)}) %all-gather.12.cloned.1.call-update) | async-done | bytes 2097168 | tf_op jit(solution)/shard_map/all_gather | solution.py:78
  186.5 6.9 convolution_convert_fusion.1
  193.5 7.9 %reduce-scatter.3.cloned.1.call-done = bf16[512,1024]{1,0:T(8,128)(2,1)} async-done(((bf16[512,2048]{1,0:T(8,128)(2,1)}), bf16[512,1024]{1,0:T(8,128)(2,1)}) %reduce-scatter.3.cloned.1.call-update) | async-done | bytes 1048592 | tf_op jit(solution)/shard_map/reduce_scatter | solution.py:81
  201.4 1.9 fusion.2
  203.3 2.5 all-reduce.1
  205.8 1.5 multiply_convert_fusion.2
  209.7 9.7 %all-gather.14.cloned.1.call-done = bf16[512,2048]{1,0:T(8,128)(2,1)} async-done(((bf16[512,1024]{1,0:T(8,128)(2,1)}), bf16[512,2048]{1,0:T(8,128)(2,1)}) %all-gather.14.cloned.1.call-update) | async-done | bytes 2097168 | tf_op jit(solution)/shard_map/all_gather | solution.py:85
  219.4 145.2 %all-gather.16.cloned.1.call-done = bf16[2048,2816]{1,0:T(8,128)(2,1)} async-done(((bf16[128,2816]{1,0:T(8,128)(2,1)}), bf16[2048,2816]{1,0:T(8,128)(2,1)}) %all-gather.16.cloned.1.call-update) | async-done | bytes 11534352 | tf_op jit(solution)/shard_map/all_gather | solution.py:90
  364.6 12.5 %fusion.50 = f32[512,2816]{1,0:T(8,128)} fusion(bf16[512,2048]{1,0:T(8,128)(2,1)} %all-gather.14.cloned.1.call-done, bf16[2048,2816]{1,0:T(8,128)(2,1)} %all-gather.16.cloned.1.call-done), kind=kOutput, calls=%fused_computation.73 | convolution fusion | flops 5905580032 | bytes 19398656 | tf_op jit(solution)/shard_map/dot_general | solution.py:30
  377.1 130.0 %all-gather.18.cloned.1.call-done = bf16[2048,2816]{1,0:T(8,128)(2,1)} async-done(((bf16[128,2816]{1,0:T(8,128)(2,1)}), bf16[2048,2816]{1,0:T(8,128)(2,1)}) %all-gather.18.cloned.1.call-update) | async-done | bytes 11534352 | tf_op jit(solution)/shard_map/all_gather | solution.py:91
  507.0 183.0 %all-gather.20.cloned.1.call-done = bf16[2816,2048]{1,0:T(8,128)(2,1)} async-done(((bf16[2816,128]{1,0:T(8,128)(2,1)}), bf16[2816,2048]{1,0:T(8,128)(2,1)}) %all-gather.20.cloned.1.call-update) | async-done | bytes 11534352 | tf_op jit(solution)/shard_map/all_gather | solution.py:95
  690.0 22.8 %convolution_convert_fusion = bf16[512,2048]{1,0:T(8,128)(2,1)} fusion(bf16[2816,2048]{1,0:T(8,128)(2,1)} %all-gather.20.cloned.1.call-done, f32[512,2816]{1,0:T(8,128)} %fusion.50, bf16[512,2048]{1,0:T(8,128)(2,1)S(1)} %copy-done.10, bf16[2048,2816]{1,0:T(8,128)(2,1)} %all-gather.18.cloned.1.call-done), kind=kOutput, calls=%fused_computation.1 | convolution fusion | flops 11820859392 | bytes 33030144 | tf_op jit(solution)/shard_map/dot_general | solution.py:93
  712.8 8.0 %reduce-scatter.5.cloned.1.call-done = bf16[512,1024]{1,0:T(8,128)(2,1)} async-done(((bf16[512,2048]{1,0:T(8,128)(2,1)}), bf16[512,1024]{1,0:T(8,128)(2,1)}) %reduce-scatter.5.cloned.1.call-update) | async-done | bytes 1048592 | tf_op jit(solution)/shard_map/reduce_scatter | solution.py:98
  720.8 1.9 fusion.3
  722.7 2.5 all-reduce
  725.2 1.5 multiply_convert_fusion.1
  (65 shorter events, 17.4 us)
Async XLA Ops:
  6.5 33.7 %copy-start.4 = (bf16[128,512]{1,0:T(8,128)(2,1)S(1)}, bf16[128,512]{1,0:T(8,128)(2,1)}, u32[]{:S(2)}) copy-start(bf16[128,512]{1,0:T(8,128)(2,1)} %param.13) | copy-start | bytes 393220
  6.5 91.2 %all-gather.8.cloned.1.call-start = ((), (), s32[]{:S(2)}) async-start(), calls=%async_computation.2 | async-start | bytes 3145728 | tf_op jit(solution)/shard_map/all_gather | solution.py:54
  7.3 114.8 %all-gather.10.cloned.1.call-start = ((), (), s32[]{:S(2)}) async-start(), calls=%async_computation.3 | async-start | bytes 2228224 | tf_op jit(solution)/shard_map/all_gather | solution.py:62
  8.0 178.5 %all-gather.12.cloned.1.call-start = ((), (), s32[]{:S(2)}) async-start(), calls=%async_computation.4 | async-start | bytes 2228224 | tf_op jit(solution)/shard_map/all_gather | solution.py:78
  8.1 10.1 %collective-permute-start = (bf16[128,512]{1,0:T(8,128)(2,1)}, bf16[128,512]{1,0:T(8,128)(2,1)S(1)}, u32[]{:S(2)}, u32[]{:S(2)}) collective-permute-start(bf16[128,512]{1,0:T(8,128)(2,1)} %param.13), channel_id=1, source_target_pairs={{0,30},{2,0},{4,2},{6,4},{8,6},{10,8},{12,10},{14,12},{16,14},{18,... | collective-permute-start | bytes 393224 | tf_op jit(solution)/shard_map/ppermute | solution.py:20
  19.1 7.2 collective-permute-start.1
  20.6 180.8 %reduce-scatter.3.cloned.1.call-start = ((), (), s32[]{:S(2)}) async-start(), calls=%async_computation.5 | async-start | bytes 3145728 | tf_op jit(solution)/shard_map/reduce_scatter | solution.py:81
  27.3 12.9 %collective-permute-start.2 = (bf16[512,512]{1,0:T(8,128)(2,1)S(1)}, bf16[512,512]{1,0:T(8,128)(2,1)S(1)}, u32[]{:S(2)}, u32[]{:S(2)}) collective-permute-start(bf16[512,512]{1,0:T(8,128)(2,1)S(1)} %pad_maximum_fusion.1), channel_id=1, source_target_pairs={{0,24},{2,26},{4,28},{6,30},{8,0},{10,2},{12,4},{14,6},{16,8},{18,... | collective-permute-start | bytes 1572872 | tf_op jit(solution)/shard_map/ppermute | solution.py:20
  40.3 52.4 %collective-permute-start.3 = (bf16[1024,512]{1,0:T(8,128)(2,1)S(1)}, bf16[1024,512]{1,0:T(8,128)(2,1)S(1)}, u32[]{:S(2)}, u32[]{:S(2)}) collective-permute-start(bf16[1024,512]{1,0:T(8,128)(2,1)S(1)} %pad_maximum_fusion), channel_id=1, source_target_pairs={{0,16},{2,18},{4,20},{6,22},{8,24},{10,26},{12,28},{14,30},{16,0},... | collective-permute-start | bytes 3145736 | tf_op jit(solution)/shard_map/ppermute | solution.py:20
  97.7 30.8 %copy-start.8 = (f32[512]{0:T(512)S(1)}, f32[512]{0:T(512)}, u32[]{:S(2)}) copy-start(f32[512]{0:T(512)} %param.15) | copy-start | bytes 6148
  125.9 3.2 copy-start.5
  125.9 3.2 copy-start.9
  193.5 8.0 %copy-start.1 = (bf16[512,1024]{1,0:T(8,128)(2,1)S(1)}, bf16[512,1024]{1,0:T(8,128)(2,1)}, u32[]{:S(2)}) copy-start(bf16[512,1024]{1,0:T(8,128)(2,1)} %param.12) | copy-start | bytes 3145732
  193.5 12.4 %copy-start.6 = (f32[1024]{0:T(1024)S(1)}, f32[1024]{0:T(1024)}, u32[]{:S(2)}) copy-start(f32[1024]{0:T(1024)} %param.19) | copy-start | bytes 12292
  193.5 25.9 %all-gather.14.cloned.1.call-start = ((), (), s32[]{:S(2)}) async-start(), calls=%async_computation.6 | async-start | bytes 3145728 | tf_op jit(solution)/shard_map/all_gather | solution.py:85
  201.4 4.4 copy-start.2
  207.4 157.2 %all-gather.16.cloned.1.call-start = ((), (), s32[]{:S(2)}) async-start(), calls=%async_computation.7 | async-start | bytes 12255232 | tf_op jit(solution)/shard_map/all_gather | solution.py:90
  207.9 299.1 %all-gather.18.cloned.1.call-start = ((), (), s32[]{:S(2)}) async-start(), calls=%async_computation.8 | async-start | bytes 12255232 | tf_op jit(solution)/shard_map/all_gather | solution.py:91
  208.7 481.3 %all-gather.20.cloned.1.call-start = ((), (), s32[]{:S(2)}) async-start(), calls=%async_computation.9 | async-start | bytes 12255232 | tf_op jit(solution)/shard_map/all_gather | solution.py:95
  209.4 511.3 %reduce-scatter.5.cloned.1.call-start = ((), (), s32[]{:S(2)}) async-start(), calls=%async_computation.10 | async-start | bytes 3145728 | tf_op jit(solution)/shard_map/reduce_scatter | solution.py:98
  219.4 470.6 %copy-start.10 = (bf16[512,2048]{1,0:T(8,128)(2,1)S(1)}, bf16[512,2048]{1,0:T(8,128)(2,1)}, u32[]{:S(2)}) copy-start(bf16[512,2048]{1,0:T(8,128)(2,1)} %all-gather.14.cloned.1.call-done) | copy-start | bytes 6291460
  712.8 8.0 %copy-start = (bf16[512,1024]{1,0:T(8,128)(2,1)S(1)}, bf16[512,1024]{1,0:T(8,128)(2,1)}, u32[]{:S(2)}) copy-start(bf16[512,1024]{1,0:T(8,128)(2,1)} %multiply_convert_fusion.2) | copy-start | bytes 3145732
  712.8 12.4 %copy-start.7 = (f32[1024]{0:T(1024)S(1)}, f32[1024]{0:T(1024)}, u32[]{:S(2)}) copy-start(f32[1024]{0:T(1024)} %param.23) | copy-start | bytes 12292
  720.8 4.4 copy-start.3
Sparse Core Ops, SparseCore 0:
  8.9 13.2 all-gather.7
  25.0 97.0 all-gather.9
  124.8 61.7 all-gather.11
  193.6 7.7 reduce-scatter.2
  207.5 11.8 all-gather.13
  222.0 142.5 all-gather.15
  367.4 139.6 all-gather.17
  509.7 180.2 all-gather.19
  712.9 7.7 reduce-scatter.4
